TPU v7x, 32 devices: a whole 2x2x4 slice. The times are simulated.
32 devices in a mesh: sp: 16 (over z, y, x), tp: 2 (over core).
Axes of the slice: x: 2, y: 2, z: 4, core: 2. Of those that a mesh axis runs over, the one named last changes fastest.
Arguments:
- tokens: bfloat16 [2048, 2048], P('sp', 'tp'), may hold values from -6 to 6
- norm_gain: float32 [2048], replicated, may hold values from 0.1 to 1.9
- w_value: bfloat16 [2048, 2048], P('sp', 'tp'), may hold values from -0.125 to 0.125
- w_gate: bfloat16 [2048, 2048], P('sp', 'tp'), may hold values from -0.125 to 0.125
- conv_taps: bfloat16 [31, 2048], P(None, 'tp'), may hold values from -1 to 1
- conv_gain: float32 [2048], P('tp'), may hold values from 0.1 to 1.9
- w_query: bfloat16 [2048, 3072], P(None, 'tp'), may hold values from -5.303301 to 5.303301
- latent_down_weight: bfloat16 [2048, 512], P('sp'), may hold values from -0.125 to 0.125
- latent_norm_gain: float32 [512], replicated, may hold values from 0.1 to 1.9
- w_rope_key: bfloat16 [2048, 64], P('sp'), may hold values from -0.125 to 0.125
- key_up_weight: bfloat16 [512, 2048], P(None, 'tp'), may hold values from -0.5 to 0.5
- value_up_weight: bfloat16 [512, 2048], P(None, 'tp'), may hold values from -0.25 to 0.25
- w_merge_conv: bfloat16 [2048, 2048], P('tp'), may hold values from -0.09375 to 0.09375
- w_merge_attn: bfloat16 [2048, 2048], P('tp'), may hold values from -0.28125 to 0.28125
Outputs:
- merged: bfloat16 [2048, 2048], P(('sp', 'tp'))
- log_sums: float32 [2048, 16], P('sp', 'tp')
All inputs are finite; a program needn't handle non-finite values.
Results may differ from a plain program's by a relative error of at most 0.025.
The roundings to bfloat16 on the way count: a program that leaves them out, or rounds other values in their place, can miss the bound.
Values may be sent and summed in bfloat16 or wider, within the bound.
A program may use at most 64 MiB of HBM per device.

v0:
```python
import jax
import jax.numpy as jnp
from jax import lax
from jax.sharding import PartitionSpec as P

PLAIN_QK_WIDTH = 128
QK_ROPE = 64
VALUE_HEAD_WIDTH = 128


epsilon = 1e-06
rope_base = 10000.0
masked_score = -1e30


def passed_along(block, axis, distance):
    devices = range(lax.axis_size(axis))
    route = [(i - distance, i) for i in devices if i - distance in devices]
    return lax.ppermute(block, axis, route)


def angles_at(positions, width):
    inverse = rope_base ** (-2.0 * jnp.arange(width // 2, dtype=jnp.float32) / width)
    return positions[:, None] * inverse[None, :]


def rotate(halves, angle):
    middle = halves.shape[-1] // 2
    first, second = (halves[..., :middle], halves[..., middle:])
    cosine, sine = (jnp.cos(angle), jnp.sin(angle))
    return jnp.concatenate(
        [first * cosine - second * sine, first * sine + second * cosine], axis=-1
    )


def local(
    tokens,
    norm_gain,
    w_value,
    w_gate,
    conv_taps,
    conv_gain,
    w_query,
    latent_down_weight,
    latent_norm_gain,
    w_rope_key,
    key_up_weight,
    value_up_weight,
    w_merge_conv,
    w_merge_attn,
):
    row_count = tokens.shape[0]
    tp_count = lax.axis_size("tp")
    gathered = lax.all_gather(tokens, "tp", axis=1, tiled=True)
    features = gathered.astype(jnp.float32)
    normed = (
        features
        * lax.rsqrt(jnp.mean(features * features, axis=-1, keepdims=True) + epsilon)
        * norm_gain
    ).astype(jnp.bfloat16)
    first_row = lax.axis_index("sp") * row_count
    query_index = first_row + jnp.arange(row_count, dtype=jnp.int32)
    slice_rows = row_count // tp_count
    slice_start = lax.axis_index("tp") * slice_rows
    key_rows = lax.dynamic_slice_in_dim(normed, slice_start, slice_rows, 0)
    key_index = first_row + slice_start + jnp.arange(slice_rows, dtype=jnp.int32)
    value_pre = jnp.dot(
        normed,
        lax.all_gather(w_value, "sp", axis=0, tiled=True),
        preferred_element_type=jnp.float32,
    )
    gate_pre = jnp.dot(
        normed, lax.all_gather(w_gate, "sp", axis=0, tiled=True), preferred_element_type=jnp.float32
    )
    latent_pre = jnp.dot(
        key_rows,
        lax.all_gather(latent_down_weight, "sp", axis=0, tiled=True),
        preferred_element_type=jnp.float32,
    )
    rope_pre = jnp.dot(
        key_rows,
        lax.all_gather(w_rope_key, "sp", axis=0, tiled=True),
        preferred_element_type=jnp.float32,
    )
    gated_rows = (value_pre * jax.nn.sigmoid(gate_pre)).astype(jnp.bfloat16)
    conv_reach = conv_taps.shape[0] - 1
    prior_rows = passed_along(gated_rows[row_count - conv_reach :], "sp", 1)
    padded = jnp.concatenate([prior_rows, gated_rows], axis=0).astype(jnp.float32)
    mixed = jnp.zeros(gated_rows.shape, jnp.float32)
    for tap_index in range(conv_taps.shape[0]):
        mixed = (
            mixed
            + conv_taps[tap_index].astype(jnp.float32) * padded[tap_index : tap_index + row_count]
        )
    channel_total = mixed.shape[1] * tp_count
    stat_sum, stat_squares = lax.psum(
        (jnp.sum(mixed, axis=1), jnp.sum(mixed * mixed, axis=1)), "tp"
    )
    channel_mean = stat_sum / channel_total
    channel_var = stat_squares / channel_total - channel_mean * channel_mean
    conv_out = jax.nn.silu(
        (mixed - channel_mean[:, None]) * lax.rsqrt(channel_var + epsilon)[:, None] * conv_gain
    ).astype(jnp.bfloat16)
    head_count = key_up_weight.shape[1] // PLAIN_QK_WIDTH
    latent_width = latent_down_weight.shape[1]
    query = (
        jnp.dot(normed, w_query, preferred_element_type=jnp.float32)
        .astype(jnp.bfloat16)
        .reshape(row_count, head_count, PLAIN_QK_WIDTH + QK_ROPE)
    )
    query_angles = angles_at(query_index.astype(jnp.float32), QK_ROPE)
    query_rope = rotate(
        query[..., PLAIN_QK_WIDTH:].astype(jnp.float32), query_angles[:, None, :]
    ).astype(jnp.bfloat16)
    key_expanded = key_up_weight.reshape(latent_width, head_count, PLAIN_QK_WIDTH)
    query_latent = jnp.einsum(
        "thd,lhd->thl",
        query[..., :PLAIN_QK_WIDTH],
        key_expanded,
        preferred_element_type=jnp.float32,
    ).astype(jnp.bfloat16)
    latent = (
        latent_pre
        * lax.rsqrt(jnp.mean(latent_pre * latent_pre, axis=-1, keepdims=True) + epsilon)
        * latent_norm_gain
    ).astype(jnp.bfloat16)
    key_rope = rotate(rope_pre, angles_at(key_index.astype(jnp.float32), QK_ROPE)).astype(
        jnp.bfloat16
    )
    score_scale = (PLAIN_QK_WIDTH + QK_ROPE) ** (-0.5)
    running_max = jnp.full((row_count, head_count), masked_score, jnp.float32)
    latent_piece = lax.all_gather(latent, ("sp", "tp"), axis=0, tiled=True)
    rope_piece = lax.all_gather(key_rope, ("sp", "tp"), axis=0, tiled=True)
    piece_rows = latent_piece.shape[0]
    scores = jnp.einsum(
        "thl,kl->thk", query_latent, latent_piece, preferred_element_type=jnp.float32
    )
    scores = (
        scores
        + jnp.einsum("thr,kr->thk", query_rope, rope_piece, preferred_element_type=jnp.float32)
    ) * score_scale
    piece_index = jnp.arange(piece_rows, dtype=jnp.int32)
    allowed = piece_index[None, None, :] <= query_index[:, None, None]
    scores = jnp.where(allowed, scores, masked_score)
    new_max = jnp.maximum(running_max, jnp.max(scores, axis=-1))
    weights = jnp.where(allowed, jnp.exp(scores - new_max[..., None]), 0.0)
    running_sum = jnp.sum(weights, axis=-1)
    weighted = jnp.einsum(
        "thk,kl->thl",
        weights.astype(jnp.bfloat16),
        latent_piece,
        preferred_element_type=jnp.float32,
    )
    running_max, running_sum, weighted = (new_max, running_sum, weighted)
    latent_result = (weighted / running_sum[..., None]).astype(jnp.bfloat16)
    log_sums = running_max + jnp.log(running_sum)
    value_expanded = value_up_weight.reshape(latent_width, head_count, VALUE_HEAD_WIDTH)
    attention = (
        jnp.einsum(
            "thl,lhv->thv", latent_result, value_expanded, preferred_element_type=jnp.float32
        )
        .astype(jnp.bfloat16)
        .reshape(row_count, head_count * VALUE_HEAD_WIDTH)
    )
    merged = lax.psum_scatter(
        (
            jnp.dot(conv_out, w_merge_conv, preferred_element_type=jnp.float32)
            + jnp.dot(attention, w_merge_attn, preferred_element_type=jnp.float32)
        ).astype(jnp.bfloat16),
        "tp",
        scatter_dimension=0,
        tiled=True,
    )
    return (merged, log_sums)


def solution(mesh):
    return jax.shard_map(
        local,
        mesh=mesh,
        in_specs=(
            P("sp", "tp"),
            P(),
            P("sp", "tp"),
            P("sp", "tp"),
            P(None, "tp"),
            P("tp"),
            P(None, "tp"),
            P("sp", None),
            P(),
            P("sp", None),
            P(None, "tp"),
            P(None, "tp"),
            P("tp", None),
            P("tp", None),
        ),
        out_specs=(P(("sp", "tp"), None), P("sp", "tp")),
        check_vma=False,
    )
```

profile of v0, /device:TPU:0, one launch (start us, length us, event | category | flops | bytes accessed | tf_op | source)
XLA Modules:
  0.0 326.8 jit_solution(12231450201018301248)
XLA Ops:
  7.2 0.7 all-gather.9.cloned.1.call-update
  8.0 0.7 all-gather.7.cloned.1.call-update
  8.7 0.7 all-gather.5.cloned.1.call-update
  9.5 44.2 %all_gather.26 = bf16[2048,64]{0,1:T(8,128)(2,1)S(1)} all-gather(bf16[128,64]{0,1:T(8,128)(2,1)} %param.23), channel_id=1, replica_groups=mesh['sp'=16,'tp'=2] {'sp'}, dimensions={0}, use_global_device_ids=true | all-gather | bytes 278528 | tf_op jit(solution)/shard_map/all_gather | solution.py:82
  53.7 2.4 all_gather.21
  56.3 0.9 fusion.18
  57.7 3.8 %convolution_convert_fusion = bf16[128,1536]{1,0:T(8,128)(2,1)S(1)} fusion(bf16[128,2048]{1,0:T(8,128)(2,1)S(1)} %fusion.18, bf16[2048,1536]{1,0:T(8,128)(2,1)} %param.20), kind=kOutput, calls=%fused_computation.10 | convolution fusion | flops 805502976 | bytes 7208960 | tf_op jit(solution)/shard_map/dot_general | solution.py:107
  61.7 12.5 %all-gather.9.cloned.1.call-done = bf16[2048,512]{1,0:T(8,128)(2,1)} async-done(((bf16[128,512]{1,0:T(8,128)(2,1)}), bf16[2048,512]{1,0:T(8,128)(2,1)}) %all-gather.9.cloned.1.call-update) | async-done | bytes 2097168 | tf_op jit(solution)/shard_map/all_gather | solution.py:77
  74.2 2.2 multiply_reduce_fusion.1
  76.4 0.7 multiply_convert_fusion.2
  77.3 0.6 slice_convert_fusion.30
  78.0 0.7 slice_convert_fusion.31
  78.7 0.7 subtract_convert_fusion
  79.6 71.8 %all-gather.7.cloned.1.call-done = bf16[2048,1024]{1,0:T(8,128)(2,1)} async-done(((bf16[128,1024]{1,0:T(8,128)(2,1)}), bf16[2048,1024]{1,0:T(8,128)(2,1)}) %all-gather.7.cloned.1.call-update) | async-done | bytes 4194320 | tf_op jit(solution)/shard_map/all_gather | solution.py:73
  151.4 3.8 %fusion.14 = f32[128,1024]{1,0:T(8,128)} fusion(bf16[128,2048]{1,0:T(8,128)(2,1)S(1)} %fusion.18, bf16[2048,1024]{1,0:T(8,128)(2,1)} %all-gather.7.cloned.1.call-done), kind=kOutput, calls=%fused_computation.23 | convolution fusion | flops 537264128 | bytes 5242880 | tf_op jit(solution)/shard_map/dot_general | solution.py:72
  155.2 73.2 %all-gather.5.cloned.1.call-done = bf16[2048,1024]{1,0:T(8,128)(2,1)} async-done(((bf16[128,1024]{1,0:T(8,128)(2,1)}), bf16[2048,1024]{1,0:T(8,128)(2,1)}) %all-gather.5.cloned.1.call-update) | async-done | bytes 4194320 | tf_op jit(solution)/shard_map/all_gather | solution.py:69
  228.4 3.0 fusion.15
  231.4 0.6 slice.276
  232.1 4.0 %collective-permute-start = (bf16[30,1024]{1,0:T(8,128)(2,1)}, bf16[30,1024]{1,0:T(8,128)(2,1)}, u32[]{:S(2)}, u32[]{:S(2)}) collective-permute-start(bf16[30,1024]{1,0:T(8,128)(2,1)} %slice.276), channel_id=1, source_target_pairs={{0,2},{2,4},{4,6},{6,8},{8,10},{10,12},{12,14},{14,16},{16,18},{18... | collective-permute-start | bytes 184328 | tf_op jit(solution)/shard_map/ppermute | solution.py:19
  236.0 38.8 %all_gather.27 = bf16[2048,64]{1,0:T(8,128)(2,1)S(1)} all-gather(bf16[64,64]{1,0:T(8,128)(2,1)S(1)} %copy.25), channel_id=1, replica_groups=mesh['sp'=16,'tp'=2] {'sp','tp'}, dimensions={0}, use_global_device_ids=true | all-gather | bytes 270336 | tf_op jit(solution)/shard_map/all_gather | solution.py:133
  274.8 1.3 copy.27
  276.1 0.9 maximum_convert_fusion
  277.1 3.9 %fusion.91 = (f32[128]{0:T(128)S(1)}, f32[128]{0:T(128)S(1)}, f32[128,1024]{1,0:T(8,128)S(1)}) fusion(f32[158,1024]{1,0:T(8,128)S(1)} %maximum_convert_fusion, f32[1024]{0:T(1024)} %bitcast.89, f32[1024]{0:T(1024)} %bitcast.90, f32[1024]{0:T(1024)} %bitcast.92, f32[1024]{0:T(1024)} %bitcast.93, f32[1024]{0:T(1024)} %bitcast.94, f32[1024]{0:T(1024)} %bitcast.95, ...), kind=kLoop, calls=%fused_computation.174 | loop fusion | flops 8388352 | bytes 16905216 | tf_op jit(solution)/shard_map/reduce_sum | solution.py:97
  281.0 2.7 all-reduce
  283.6 4.1 %fusion.62 = f32[128,2048]{1,0:T(8,128)} fusion(bf16[1024,2048]{1,0:T(8,128)(2,1)} %param.26, f32[128,1024]{1,0:T(8,128)S(1)} %get-tuple-element.6, f32[1024]{0:T(1024)S(1)} %copy-done.8, f32[128]{0:T(128)S(1)} %get-tuple-element.45, f32[128]{0:T(128)S(1)} %get-tuple-element.44), kind=kOutput, calls=%fused_computation.97 | convolution fusion | flops 537919488 | bytes 5772288 | tf_op jit(solution)/shard_map/dot_general | solution.py:167
  287.8 7.6 %fusion.9 = f32[128,8,2048]{2,0,1:T(8,128)} fusion(bf16[2048,512]{1,0:T(8,128)(2,1)} %all-gather.11.cloned.1.call-done, bf16[128,8,192]{0,2,1:T(8,128)(2,1)S(1)} %bitcast.77, bf16[512,1024]{1,0:T(8,128)(2,1)S(1)} %copy-done), kind=kOutput, calls=%fused_computation.12 | convolution fusion | flops 2282225664 | bytes 11796480 | tf_op jit(solution)/shard_map/thl,kl->thk/dot_general | solution.py:135
  295.3 5.5 %fusion.93 = (f32[128,8]{0,1:T(8,128)S(1)}, f32[128,8,2048]{2,0,1:T(8,128)S(1)}) fusion(f32[128,8,2048]{2,0,1:T(8,128)} %fusion.9, bf16[2048,64]{1,0:T(8,128)(2,1)S(1)} %all_gather.27, bf16[128,8,32]{0,2,1:T(8,128)(2,1)S(1)} %copy-done.5, bf16[128,8,32]{0,2,1:T(8,128)(2,1)S(1)} %copy-done.4, pred[128,2048]{1,0:T(8,128)(4,1)S(1)} %iota_compare_fusion), kind=kOutput, calls=%fused_computation.175 | convolution fusion | flops 277085184 | bytes 17436672 | tf_op jit(solution)/shard_map/thr,kr->thk/dot_general | solution.py:140
  300.8 2.0 fusion
  302.9 1.2 copy-done.1
  304.0 6.7 %convolution_convert_fusion.2 = bf16[8,128,128]{1,2,0:T(8,128)(2,1)S(1)} fusion(bf16[512,8,128]{0,2,1:T(8,128)(2,1)S(1)} %bitcast.75, f32[128,8]{0,1:T(8,128)S(1)} %fusion, f32[128,8,2048]{2,0,1:T(8,128)} %copy-done.1, f32[128,8]{0,1:T(8,128)S(1)} %broadcast_maximum_fusion, pred[128,2048]{1,0:T(8,128)(4,1)S(1)} %iota_compare_fusion, ...), kind=kOutput, calls=%fused_computation.24 | convolution fusion | flops 2289172480 | bytes 12066816 | tf_op jit(solution)/shard_map/thl,lhv->thv/dot_general | solution.py:159
  310.7 4.0 %fusion.7 = bf16[128,2048]{1,0:T(8,128)(2,1)} fusion(f32[128,2048]{1,0:T(8,128)} %fusion.62, bf16[128,1024]{0,1:T(8,128)(2,1)S(1)} %bitcast.78, bf16[1024,2048]{1,0:T(8,128)(2,1)} %param.27), kind=kOutput, calls=%fused_computation.9 | convolution fusion | flops 537395200 | bytes 6029312 | tf_op jit(solution)/shard_map/dot_general | solution.py:168
  315.4 5.0 %reduce-scatter.2.cloned.1.call-done = bf16[64,2048]{1,0:T(8,128)(2,1)} async-done(((bf16[128,2048]{1,0:T(8,128)(2,1)}), bf16[64,2048]{1,0:T(8,128)(2,1)}) %reduce-scatter.2.cloned.1.call-update) | async-done | bytes 262160 | tf_op jit(solution)/shard_map/reduce_scatter | solution.py:165
  (44 shorter events, 2.2 us)
Async XLA Ops:
  7.2 280.6 %copy-start = (bf16[512,1024]{1,0:T(8,128)(2,1)S(1)}, bf16[512,1024]{1,0:T(8,128)(2,1)}, u32[]{:S(2)}) copy-start(bf16[512,1024]{1,0:T(8,128)(2,1)} %param.24) | copy-start | bytes 3145732
  7.2 67.0 %all-gather.9.cloned.1.call-start = ((), (), s32[]{:S(2)}) async-start(), calls=%async_computation.3 | async-start | bytes 2228224 | tf_op jit(solution)/shard_map/all_gather | solution.py:77
  7.9 143.5 %all-gather.7.cloned.1.call-start = ((), (), s32[]{:S(2)}) async-start(), calls=%async_computation.2 | async-start | bytes 4456448 | tf_op jit(solution)/shard_map/all_gather | solution.py:73
  8.7 219.7 %all-gather.5.cloned.1.call-start = ((), (), s32[]{:S(2)}) async-start(), calls=%async_computation.1 | async-start | bytes 4456448 | tf_op jit(solution)/shard_map/all_gather | solution.py:69
  9.4 278.4 %all-gather.11.cloned.1.call-start = ((), (), s32[]{:S(2)}) async-start(), calls=%async_computation.4 | async-start | bytes 2162688 | tf_op jit(solution)/shard_map/all_gather | solution.py:132
  57.6 18.7 %copy-start.7 = (f32[512]{0:T(512)S(1)}, f32[512]{0:T(512)}, u32[]{:S(2)}) copy-start(f32[512]{0:T(512)} %param.22) | copy-start | bytes 6148
  57.7 19.7 %copy-start.6 = (bf16[31,1024]{1,0:T(8,128)(2,1)S(1)}, bf16[31,1024]{1,0:T(8,128)(2,1)}, u32[]{:S(2)}) copy-start(bf16[31,1024]{1,0:T(8,128)(2,1)} %param.18) | copy-start | bytes 190468
  77.1 243.2 %reduce-scatter.2.cloned.1.call-start = ((), (), s32[]{:S(2)}) async-start(), calls=%async_computation.5 | async-start | bytes 786432 | tf_op jit(solution)/shard_map/reduce_scatter | solution.py:165
  155.2 119.7 %copy-start.2 = (bf16[512,1024]{1,0:T(8,128)(2,1)S(1)}, bf16[512,1024]{1,0:T(8,128)(2,1)}, u32[]{:S(2)}) copy-start(bf16[512,1024]{1,0:T(8,128)(2,1)} %param.25) | copy-start | bytes 3145732
  232.1 44.1 %collective-permute-start = (bf16[30,1024]{1,0:T(8,128)(2,1)}, bf16[30,1024]{1,0:T(8,128)(2,1)}, u32[]{:S(2)}, u32[]{:S(2)}) collective-permute-start(bf16[30,1024]{1,0:T(8,128)(2,1)} %slice.276), channel_id=1, source_target_pairs={{0,2},{2,4},{4,6},{6,8},{8,10},{10,12},{12,14},{14,16},{16,18},{18... | collective-permute-start | bytes 184328 | tf_op jit(solution)/shard_map/ppermute | solution.py:19
  277.1 6.6 %copy-start.8 = (f32[1024]{0:T(1024)S(1)}, f32[1024]{0:T(1024)}, u32[]{:S(2)}) copy-start(f32[1024]{0:T(1024)} %param.19) | copy-start | bytes 12292
  287.8 7.6 %copy-start.4 = (bf16[128,8,32]{0,2,1:T(8,128)(2,1)S(1)}, bf16[128,8,32]{0,2,1:T(8,128)(2,1)}, u32[]{:S(2)}) copy-start(bf16[128,8,32]{0,2,1:T(8,128)(2,1)} %get-tuple-element.7) | copy-start | bytes 196612
  287.8 7.6 %copy-start.5 = (bf16[128,8,32]{0,2,1:T(8,128)(2,1)S(1)}, bf16[128,8,32]{0,2,1:T(8,128)(2,1)}, u32[]{:S(2)}) copy-start(bf16[128,8,32]{0,2,1:T(8,128)(2,1)} %get-tuple-element.8) | copy-start | bytes 196612
  300.8 3.2 copy-start.1
  300.8 3.2 copy-start.3
Sparse Core Ops, SparseCore 0:
  10.8 63.3 all-gather.8
  76.9 74.4 all-gather.6
  154.2 74.1 all-gather.4
  231.1 55.2 all-gather.10
  314.9 5.3 reduce-scatter.1
where the time goes:
time: 327 us
  waiting for transfers between devices  165 us (50%)
  blocking collectives  88 us (27%)
  matrix products  40.8 us (12%)
  between operations  14 us (4%)
  other arithmetic  11.8 us (4%)
  starting transfers between devices  4.15 us (1%)
  local copies, waits for them, and re-layouts  3.47 us (1%)
    all_gather x1, waiting for transfers between devices, local(): lax.all_gather(w_value, 'sp', axis=0, tiled=True)  73.2 us
    all_gather x1, waiting for transfers between devices, local(): lax.all_gather(w_gate, 'sp', axis=0, tiled=True)  71.8 us
    all_gather x1, blocking collectives, local(): lax.all_gather(w_rope_key, 'sp', axis=0, tiled=True)  44.2 us
    all_gather x1, blocking collectives, local(): rope_piece = lax.all_gather(key_rope, ('sp', 'tp'), axis=0, tiled=True)  38.8 us
    all_gather x1, waiting for transfers between devices, local(): lax.all_gather(latent_down_weight, 'sp', axis=0, tiled=True)  12.5 us
    dot_general x1, matrix products, local(): jnp.einsum('thl,kl->thk', query_latent, latent_piece, preferred_element_t...  7.56 us
    dot_general x1, matrix products, local(): jnp.einsum('thl,lhv->thv', latent_result, value_expanded, preferred_eleme...  6.65 us
  transfers between devices with their start and end apart: 6, of which 4 were waited for; matrix products, arithmetic and copies ran while one was open for 9% of the time, Pallas kernels for 0%

commit v1 on v0

v1 whole, which is shorter than its diff:
```python
import jax
import jax.numpy as jnp
from jax import lax
from jax.experimental import pallas as pl
from jax.experimental.pallas import tpu as pltpu
from jax.sharding import PartitionSpec as P

PLAIN_QK_WIDTH = 128
QK_ROPE = 64
VALUE_HEAD_WIDTH = 128

epsilon = 1e-06
rope_base = 10000.0
masked_score = -1e30
MESH = pl.DeviceIdType.MESH
ANY = pl.BlockSpec(memory_space=pl.ANY)


def angles_at(positions, width):
    inverse = rope_base ** (-2.0 * jnp.arange(width // 2, dtype=jnp.float32) / width)
    return positions[:, None] * inverse[None, :]


def rotate(halves, angle):
    middle = halves.shape[-1] // 2
    first, second = (halves[..., :middle], halves[..., middle:])
    cosine, sine = (jnp.cos(angle), jnp.sin(angle))
    return jnp.concatenate(
        [first * cosine - second * sine, first * sine + second * cosine], axis=-1
    )


class Place:
    def __init__(self, sp, tp, B):
        self.sp, self.tp, self.B, self.A = sp, tp, B, sp // B
        self.s = lax.axis_index("sp")
        self.t = lax.axis_index("tp")
        self.a = self.s // B
        self.b = lax.rem(self.s, B)

    def in_line(self, k):
        return {"sp": lax.rem(self.a + k, self.A) * self.B + self.b, "tp": self.t}

    def in_plane(self, k):
        return {"sp": self.a * self.B + lax.rem(self.b + k, self.B), "tp": self.t}

    def in_sp(self, k):
        return {"sp": lax.rem(self.s + k, self.sp), "tp": self.t}

    def in_tp(self, k):
        return {"sp": self.s, "tp": lax.rem(self.t + k, self.tp)}


def loop(start, stop, body):
    if stop > start:
        lax.fori_loop(start, stop, lambda k, c: (body(k), c)[1], 0)


def greet(groups):
    barrier = pltpu.get_barrier_semaphore()
    total = 0
    for where, count in groups:
        loop(
            1,
            count,
            lambda k: pl.semaphore_signal(
                barrier, inc=1, device_id=where(k), device_id_type=MESH
            ),
        )
        total += count - 1
    pl.semaphore_wait(barrier, total)


def remote(src, dst, send, recv, where):
    return pltpu.make_async_remote_copy(
        src_ref=src, dst_ref=dst, send_sem=send, recv_sem=recv, device_id=where,
        device_id_type=MESH,
    )


def stages(p, out, send, recv):
    line = lambda k: remote(
        out.at[p.a, p.b, p.t], out.at[p.a, p.b, p.t],
        send.at[0, k], recv.at[0, k], p.in_line(k))
    plane = lambda k: remote(
        out.at[:, p.b, p.t], out.at[:, p.b, p.t],
        send.at[1, k], recv.at[1, k], p.in_plane(k))
    pair = lambda k: remote(
        out.at[:, :, p.t], out.at[:, :, p.t],
        send.at[2, k], recv.at[2, k], p.in_tp(k))
    return line, plane, pair


def first_kernel(sp, tp, B, tok, wv, wg, wd, x, vo, go, do, local, tsend, trecv,
                 dsend, drecv, wsend, wrecv):
    p = Place(sp, tp, B)
    F = tok.shape[1]
    width = vo.shape[2]
    mine = pl.ds(pl.multiple_of(p.t * F, F), F)
    columns = lambda k: pl.ds(
        pl.multiple_of(lax.rem(lax.rem(p.s + k, sp), B) * width, width), width)
    greet([(p.in_sp, sp), (p.in_tp, tp)])
    own = [
        pltpu.make_async_copy(wd, do.at[p.a, p.b, p.t], local.at[0]),
        pltpu.make_async_copy(tok, x.at[p.b, :, mine], local.at[1]),
        pltpu.make_async_copy(wv.at[:, columns(0)], vo.at[p.s], local.at[2]),
        pltpu.make_async_copy(wg.at[:, columns(0)], go.at[p.s], local.at[3]),
    ]
    for copy in own:
        copy.start()
    tok_plane = lambda k: remote(
        tok, x.at[p.b, :, mine], tsend.at[0, k], trecv.at[0, k], p.in_plane(k))
    tok_pair = lambda k: remote(
        x.at[:, :, mine], x.at[:, :, mine], tsend.at[1, k], trecv.at[1, k], p.in_tp(k))
    value = lambda k: remote(
        wv.at[:, columns(k)], vo.at[p.s], wsend.at[0, k], wrecv.at[0, k], p.in_sp(k))
    gate = lambda k: remote(
        wg.at[:, columns(k)], go.at[p.s], wsend.at[1, k], wrecv.at[1, k], p.in_sp(k))
    line, plane, pair = stages(p, do, dsend, drecv)
    own[0].wait()
    loop(1, p.A, lambda k: line(k).start())
    loop(1, B, lambda k: tok_plane(k).start())
    loop(1, sp, lambda k: value(k).start())
    loop(1, p.A, lambda k: line(k).wait())
    loop(1, B, lambda k: plane(k).start())
    loop(1, sp, lambda k: gate(k).start())
    own[1].wait()
    loop(1, B, lambda k: tok_plane(k).wait())
    loop(1, tp, lambda k: tok_pair(k).start())
    loop(1, B, lambda k: plane(k).wait())
    loop(1, tp, lambda k: pair(k).start())
    loop(1, sp, lambda k: value(k).wait())
    loop(1, sp, lambda k: gate(k).wait())
    loop(1, tp, lambda k: tok_pair(k).wait())
    loop(1, tp, lambda k: pair(k).wait())
    own[2].wait()
    own[3].wait()


def gather_first(sp, tp, B, tok, wv, wg, wd):
    R, F = tok.shape
    D, C = wv.shape
    sds = jax.ShapeDtypeStruct
    D2 = pltpu.SemaphoreType.DMA
    most = max(sp // B, B, tp)
    return pl.pallas_call(
        lambda *refs: first_kernel(sp, tp, B, *refs),
        out_shape=(
            sds((B, R, tp * F), tok.dtype),
            sds((sp, D, C // B), wv.dtype),
            sds((sp, D, C // B), wg.dtype),
            sds((sp // B, B, tp) + wd.shape, wd.dtype),
        ),
        in_specs=[ANY] * 4,
        out_specs=(ANY,) * 4,
        scratch_shapes=[
            D2((4,)), D2((2, max(B, tp))), D2((2, max(B, tp))),
            D2((3, most)), D2((3, most)), D2((2, sp)), D2((2, sp)),
        ],
        compiler_params=pltpu.CompilerParams(collective_id=0, has_side_effects=True),
        name="gather_first",
    )(tok, wv, wg, wd)


def latent_kernel(sp, tp, B, block, out, local, send, recv):
    p = Place(sp, tp, B)
    greet([(p.in_line, p.A), (p.in_plane, B), (p.in_tp, tp)])
    own = pltpu.make_async_copy(block, out.at[p.a, p.b, p.t], local)
    own.start()
    own.wait()
    for part, count in zip(stages(p, out, send, recv), (p.A, B, tp)):
        loop(1, count, lambda k: part(k).start())
        loop(1, count, lambda k: part(k).wait())


def gather_latent(sp, tp, B, block):
    most = max(sp // B, B, tp)
    D2 = pltpu.SemaphoreType.DMA
    return pl.pallas_call(
        lambda *refs: latent_kernel(sp, tp, B, *refs),
        out_shape=jax.ShapeDtypeStruct((sp // B, B, tp) + block.shape, block.dtype),
        in_specs=[ANY],
        out_specs=ANY,
        scratch_shapes=[D2(()), D2((3, most)), D2((3, most))],
        compiler_params=pltpu.CompilerParams(collective_id=1, has_side_effects=True),
        name="gather_latent",
    )(block)


def swap_kernel(sp, tp, B, plane, blocks, out, local, send, recv):
    p = Place(sp, tp, B)
    n = B if plane else tp
    me = p.b if plane else p.t
    where = p.in_plane if plane else p.in_tp
    greet([(where, n)])
    own = pltpu.make_async_copy(blocks.at[me], out.at[me], local)
    own.start()
    copy = lambda k: remote(
        blocks.at[lax.rem(me + k, n)], out.at[me], send.at[k], recv.at[k], where(k))
    loop(1, n, lambda k: copy(k).start())
    loop(1, n, lambda k: copy(k).wait())
    own.wait()


def swap(sp, tp, B, plane, blocks, collective_id):
    D2 = pltpu.SemaphoreType.DMA
    n = B if plane else tp
    return pl.pallas_call(
        lambda *refs: swap_kernel(sp, tp, B, plane, *refs),
        out_shape=jax.ShapeDtypeStruct(blocks.shape, blocks.dtype),
        in_specs=[ANY],
        out_specs=ANY,
        scratch_shapes=[D2(()), D2((n,)), D2((n,))],
        compiler_params=pltpu.CompilerParams(
            collective_id=collective_id, has_side_effects=True),
        name="swap_plane" if plane else "swap_tp",
    )(blocks)


def norm_rows(features, gain):
    return (
        features
        * lax.rsqrt(jnp.mean(features * features, axis=-1, keepdims=True) + epsilon)
        * gain
    ).astype(jnp.bfloat16)


def local(
    tokens,
    norm_gain,
    w_value,
    w_gate,
    conv_taps,
    conv_gain,
    w_query,
    latent_down_weight,
    latent_norm_gain,
    w_rope_key,
    key_up_weight,
    value_up_weight,
    w_merge_conv,
    w_merge_attn,
):
    row_count = tokens.shape[0]
    sp = lax.axis_size("sp")
    tp = lax.axis_size("tp")
    C = w_value.shape[1]
    B = 1
    while B < 4 and sp % (2 * B) == 0 and C % (2 * B * 128) == 0:
        B *= 2
    s, t = lax.axis_index("sp"), lax.axis_index("tp")
    spot = lax.rem(s, B)
    latent_width = latent_down_weight.shape[1]

    down = jnp.concatenate([latent_down_weight, w_rope_key], axis=1)
    down_rows = down.shape[0] // tp
    down = lax.dynamic_slice_in_dim(down, t * down_rows, down_rows, 0)
    x, value_w, gate_w, down_w = gather_first(sp, tp, B, tokens, w_value, w_gate, down)
    features = x.shape[-1]
    x = x.reshape(B * row_count, features)
    normed = norm_rows(x.astype(jnp.float32), norm_gain)
    own = lax.dynamic_slice_in_dim(normed, spot * row_count, row_count, 0)
    first_row = s * row_count
    query_index = first_row + jnp.arange(row_count, dtype=jnp.int32)
    slice_rows = row_count // tp
    slice_start = t * slice_rows
    key_rows = lax.dynamic_slice_in_dim(own, slice_start, slice_rows, 0)
    key_index = first_row + slice_start + jnp.arange(slice_rows, dtype=jnp.int32)
    down_pre = jnp.dot(
        key_rows, down_w.reshape(features, -1), preferred_element_type=jnp.float32
    )
    latent = norm_rows(down_pre[:, :latent_width], latent_norm_gain)
    key_rope = rotate(
        down_pre[:, latent_width:], angles_at(key_index.astype(jnp.float32), QK_ROPE)
    ).astype(jnp.bfloat16)
    keys = gather_latent(sp, tp, B, jnp.concatenate([latent, key_rope], axis=1))
    keys = keys.reshape(sp * row_count, -1)

    value_pre = jnp.dot(
        normed, value_w.reshape(features, -1), preferred_element_type=jnp.float32
    )
    gate_pre = jnp.dot(
        normed, gate_w.reshape(features, -1), preferred_element_type=jnp.float32
    )
    gated = (value_pre * jax.nn.sigmoid(gate_pre)).astype(jnp.bfloat16)
    rows, width = gated.shape
    reach = conv_taps.shape[0] - 1
    prior, back = [], 1
    while sum(q.shape[0] for q in prior) < reach:
        need = min(rows, reach - sum(q.shape[0] for q in prior))
        route = [(i - back * B, i) for i in range(back * B, sp)]
        prior.insert(0, lax.ppermute(gated[rows - need :], "sp", route))
        back += 1
    padded = jnp.concatenate(prior + [gated], axis=0).astype(jnp.float32)
    taps = lax.dynamic_slice_in_dim(conv_taps, spot * width, width, 1).astype(jnp.float32)
    mixed = jnp.zeros(gated.shape, jnp.float32)
    for tap_index in range(reach + 1):
        mixed = mixed + taps[tap_index] * padded[tap_index : tap_index + rows]
    mixed = swap(sp, tp, B, True, mixed.astype(jnp.bfloat16).reshape(B, row_count, width), 2)
    mixed = mixed.astype(jnp.float32)
    stat_sum, stat_squares = lax.psum(
        (jnp.sum(mixed, axis=(0, 2)), jnp.sum(mixed * mixed, axis=(0, 2))), "tp"
    )
    channel_total = C * tp
    channel_mean = stat_sum / channel_total
    channel_var = stat_squares / channel_total - channel_mean * channel_mean
    conv_out = jax.nn.silu(
        (mixed - channel_mean[None, :, None])
        * lax.rsqrt(channel_var + epsilon)[None, :, None]
        * conv_gain.reshape(B, 1, width)
    ).astype(jnp.bfloat16)

    head_count = key_up_weight.shape[1] // PLAIN_QK_WIDTH
    query = (
        jnp.dot(own, w_query, preferred_element_type=jnp.float32)
        .astype(jnp.bfloat16)
        .reshape(row_count, head_count, PLAIN_QK_WIDTH + QK_ROPE)
    )
    query_angles = angles_at(query_index.astype(jnp.float32), QK_ROPE)
    query_rope = rotate(
        query[..., PLAIN_QK_WIDTH:].astype(jnp.float32), query_angles[:, None, :]
    ).astype(jnp.bfloat16)
    key_expanded = key_up_weight.reshape(latent_width, head_count, PLAIN_QK_WIDTH)
    query_latent = jnp.einsum(
        "thd,lhd->thl",
        query[..., :PLAIN_QK_WIDTH],
        key_expanded,
        preferred_element_type=jnp.float32,
    ).astype(jnp.bfloat16)
    score_scale = (PLAIN_QK_WIDTH + QK_ROPE) ** (-0.5)
    scores = (
        jnp.einsum(
            "thl,kl->thk",
            jnp.concatenate([query_latent, query_rope], axis=-1),
            keys,
            preferred_element_type=jnp.float32,
        )
        * score_scale
    )
    key_at = jnp.arange(keys.shape[0], dtype=jnp.int32)
    allowed = key_at[None, None, :] <= query_index[:, None, None]
    scores = jnp.where(allowed, scores, masked_score)
    row_max = jnp.max(scores, axis=-1)
    weights = jnp.where(allowed, jnp.exp(scores - row_max[..., None]), 0.0)
    weight_sum = jnp.sum(weights, axis=-1)
    weighted = jnp.einsum(
        "thk,kl->thl",
        weights.astype(jnp.bfloat16),
        keys[:, :latent_width],
        preferred_element_type=jnp.float32,
    )
    latent_result = (weighted / weight_sum[..., None]).astype(jnp.bfloat16)
    log_sums = row_max + jnp.log(weight_sum)
    value_expanded = value_up_weight.reshape(latent_width, head_count, VALUE_HEAD_WIDTH)
    attention = (
        jnp.einsum(
            "thl,lhv->thv", latent_result, value_expanded, preferred_element_type=jnp.float32
        )
        .astype(jnp.bfloat16)
        .reshape(row_count, head_count * VALUE_HEAD_WIDTH)
    )
    partial = (
        jnp.einsum(
            "btc,bcm->tm",
            conv_out,
            w_merge_conv.reshape(B, width, -1),
            preferred_element_type=jnp.float32,
        )
        + jnp.dot(attention, w_merge_attn, preferred_element_type=jnp.float32)
    ).astype(jnp.bfloat16)
    parts = swap(sp, tp, B, False, partial.reshape(tp, slice_rows, -1), 3)
    merged = jnp.sum(parts.astype(jnp.float32), axis=0).astype(jnp.bfloat16)
    return (merged, log_sums)


def solution(mesh):
    return jax.shard_map(
        local,
        mesh=mesh,
        in_specs=(
            P("sp", "tp"),
            P(),
            P("sp", "tp"),
            P("sp", "tp"),
            P(None, "tp"),
            P("tp"),
            P(None, "tp"),
            P("sp", None),
            P(),
            P("sp", None),
            P(None, "tp"),
            P(None, "tp"),
            P("tp", None),
            P("tp", None),
        ),
        out_specs=(P(("sp", "tp"), None), P("sp", "tp")),
        check_vma=False,
    )
```

time: 327 us -> 175 us (0.54)
  waiting for transfers between devices: 165 us -> 0.01 us
  Pallas kernels: 0 us -> 114 us
  blocking collectives: 88 us -> 2.47 us
  matrix products: 40.8 us -> 26.4 us
  between operations: 14 us -> 1.48 us
  other arithmetic: 11.8 us -> 21.2 us
  local copies, waits for them, and re-layouts: 3.47 us -> 7.34 us
    all_gather x4 -> x0, waiting for transfers between devices: 158 us -> none  [the longest x1 73.2 us: local(): lax.all_gather(w_value, 'sp', axis=0, tiled=True)]
    pallas_call x0 -> x4, Pallas kernels: none -> 114 us  [the longest x1 64.7 us: gather_first(): pl.pallas_call(lambda *refs: first_kernel(sp, tp, B, *refs), out_shape=(s...]
    all_gather x3 -> x0, blocking collectives: 85.4 us -> none  [the longest x1 44.2 us: local(): lax.all_gather(w_rope_key, 'sp', axis=0, tiled=True)]
    dot_general x8 -> x7, matrix products: 30.1 us -> 18.2 us  [the longest x1 5.58 us: local(): jnp.einsum('thl,kl->thk', jnp.concatenate([query_latent, query_rope], axi...]
    convert_element_type x4 -> x6, other arithmetic: 2.52 us -> 7.95 us  [the longest x3 4.2 us: norm_rows(): return (features * lax.rsqrt(jnp.mean(features * features, axis=-1, keepd...]
    reduce_scatter x1 -> x0, waiting for transfers between devices: 4.96 us -> none  [local(): lax.psum_scatter((jnp.dot(conv_out, w_merge_conv, preferred_element_type=...]
    reduce_sum x3 -> x5, other arithmetic: 6.1 us -> 7.81 us  [the longest x1 2.54 us: local(): weight_sum = jnp.sum(weights, axis=-1)]
  transfers between devices with their start and end apart: 6 -> 1, of which waited for: 4 -> 0; matrix products, arithmetic and copies ran while one was open for 9% -> 19% of each run, Pallas kernels for 0% -> 19%
where the time goes in v1:
time: 175 us; the launch traced here: 174 us
  Pallas kernels  114 us (65%)
  matrix products  26.4 us (15%)
  other arithmetic  21.2 us (12%)
  local copies, waits for them, and re-layouts  7.34 us (4%)
  blocking collectives  2.47 us (1%)
  starting transfers between devices  1.75 us (1%)
    pallas_call x1, Pallas kernels, gather_first(): pl.pallas_call(lambda *refs: first_kernel(sp, tp, B, *refs), out_shape=(s...  64.7 us
    pallas_call x1, Pallas kernels, gather_latent(): pl.pallas_call(lambda *refs: latent_kernel(sp, tp, B, *refs), out_shape=j...  33 us
    pallas_call x2, Pallas kernels, swap(): pl.pallas_call(lambda *refs: swap_kernel(sp, tp, B, plane, *refs), out_sh...  16.1 us
    dot_general x1, matrix products, local(): jnp.einsum('thl,lhv->thv', latent_result, value_expanded, preferred_eleme...  6.69 us
    dot_general x1, matrix products, local(): jnp.einsum('thl,kl->thk', jnp.concatenate([query_latent, query_rope], axi...  5.58 us
    convert_element_type x3, other arithmetic, norm_rows(): return (features * lax.rsqrt(jnp.mean(features * features, axis=-1, keepd...  4.2 us
    dot_general x1, matrix products, local(): jnp.dot(own, w_query, preferred_element_type=jnp.float32)  3.97 us
  transfers between devices with their start and end apart: 1, of which 0 were waited for; matrix products, arithmetic and copies ran while one was open for 19% of the time, Pallas kernels for 19%

profile of v1, /device:TPU:0, one launch (start us, length us, event | category | flops | bytes accessed | tf_op | source)
XLA Modules:
  0.0 174.3 jit_solution(12513168388297866614)
XLA Ops:
  0.7 0.9 copy.24
  1.6 1.5 fusion.75.refs_3_
  3.1 64.7 %gather_first.1 = (bf16[4,128,2048]{2,1,0:T(8,128)(2,1)}, bf16[16,128,256]{2,1,0:T(8,128)(2,1)}, bf16[16,128,256]{2,1,0:T(8,128)(2,1)}, bf16[4,4,2,64,576]{4,3,2,1,0:T(8,128)(2,1)}) custom-call(bf16[128,1024]{1,0:T(8,128)(2,1)} %refs_0_.1, bf16[128,1024]{1,0:T(8,128)(2,1)} %refs_1_.1, bf16[128,1024]{1,0:T(8,128)(2,1)} %refs_2_.1, bf16[64,576]{1,0:T(8,128)(2,1)} %fusion.75.refs_3_), custom_call_target="tpu_custom_call" | custom-call | tf_op jit(solution)/shard_map/gather_first/pallas_call | solution.py:146
  67.8 2.2 %multiply_reduce_fusion = f32[4,128]{1,0:T(4,128)S(1)} fusion(bf16[4,128,2048]{2,1,0:T(8,128)(2,1)} %get-tuple-element.6), kind=kLoop, calls=%fused_computation.9 | loop fusion | flops 3145216 | bytes 2099200 | tf_op jit(solution)/shard_map/reduce_sum | solution.py:223
  69.9 2.2 %multiply_convert_fusion = bf16[4,128,2048]{2,1,0:T(8,128)(2,1)S(1)} fusion(f32[2048]{0:T(1024)} %param.15, f32[4,128]{1,0:T(4,128)S(1)} %get-tuple-element.50, bf16[4,128,2048]{2,1,0:T(8,128)(2,1)} %get-tuple-element.6), kind=kLoop, calls=%fused_computation.8 | loop fusion | flops 4194304 | bytes 4204544 | tf_op jit(solution)/shard_map/convert_element_type | solution.py:225
  72.2 0.7 fusion.18
  73.0 0.7 fusion.19
  73.7 0.7 copy-done.6
  75.0 1.8 %collective-permute-start = (bf16[30,256]{1,0:T(8,128)(2,1)}, bf16[30,256]{1,0:T(8,128)(2,1)S(1)}, u32[]{:S(2)}, u32[]{:S(2)}) collective-permute-start(bf16[30,256]{1,0:T(8,128)(2,1)} %slice.288), channel_id=1, source_target_pairs={{0,8},{2,10},{4,12},{6,14},{8,16},{10,18},{12,20},{14,22},{16,24},... | collective-permute-start | bytes 46088 | tf_op jit(solution)/shard_map/ppermute | solution.py:292
  77.8 0.7 dynamic-slice_convert_fusion
  78.5 0.6 fusion.97
  79.2 0.7 fusion.96
  80.6 2.3 %copy.36 = bf16[512,1024]{0,1:T(8,128)(2,1)} copy(bf16[512,1024]{1,0:T(8,128)(2,1)} %param.25) | data formatting | bytes 2097152 | tf_op jit(solution)/shard_map/reshape | solution.py:354
  82.9 1.9 %fusion.4 = bf16[512,2048]{1,0:T(8,128)(2,1)} fusion(f32[2048]{0:T(1024)S(1)} %copy-done.8, f32[512]{0:T(512)S(1)} %get-tuple-element.49, bf16[4,128,2048]{2,1,0:T(8,128)(2,1)S(1)} %copy-done.1), kind=kLoop, calls=%fused_computation.7 | loop fusion | flops 4194304 | bytes 4204544 | tf_op jit(solution)/shard_map/convert_element_type | solution.py:225
  84.8 4.0 %convolution_convert_fusion = bf16[128,1536]{1,0:T(8,128)(2,1)S(1)} fusion(bf16[2048,1536]{1,0:T(8,128)(2,1)} %param.20, bf16[512,2048]{1,0:T(8,128)(2,1)} %fusion.4, s32[]{:T(128)S(6)} %select_n.23), kind=kOutput, calls=%fused_computation.15 | convolution fusion | flops 805502976 | bytes 7208964 | tf_op jit(solution)/shard_map/dot_general | solution.py:315
  89.0 2.4 %fusion.69 = f32[64,576]{1,0:T(8,128)S(1)} fusion(bf16[2048,576]{1,0:T(8,128)(2,1)} %bitcast.83, bf16[512,2048]{1,0:T(8,128)(2,1)} %fusion.4, s32[]{:T(128)S(6)} %dynamic_slice.18), kind=kOutput, calls=%fused_computation.115 | convolution fusion | flops 150994944 | bytes 3031044 | tf_op jit(solution)/shard_map/dot_general | solution.py:269
  92.3 1.5 fusion.9
  93.9 0.7 pad_maximum_fusion.refs_0_
  94.6 33.0 %gather_latent.1 = bf16[4,4,2,64,576]{4,3,2,1,0:T(8,128)(2,1)} custom-call(bf16[64,576]{1,0:T(8,128)(2,1)} %pad_maximum_fusion.refs_0_), custom_call_target="tpu_custom_call" | custom-call | tf_op jit(solution)/shard_map/gather_latent/pallas_call | solution.py:179
  127.9 5.6 %fusion = (f32[128,8]{0,1:T(8,128)S(1)}, f32[128,8,2048]{2,0,1:T(8,128)S(1)}) fusion(pred[128,2048]{1,0:T(8,128)(4,1)S(1)} %iota_compare_fusion, bf16[2048,576,1]{1,0,2:T(8,128)(2,1)} %bitcast.84, bf16[128,8,32]{2,0,1:T(8,128)(2,1)S(1)} %get-tuple-element.15, bf16[128,8,32]{2,0,1:T(8,128)(2,1)S(1)} %get-tuple-element.14, bf16[128,8,512]{2,0,1:T(8,128)(2,1)S(1)} %copy-done.5), kind=kOutput, calls=%fused_computation.2 | convolution fusion | flops 2425748480 | bytes 12193792 | tf_op jit(solution)/shard_map/thl,kl->thk/dot_general | solution.py:332
  133.5 2.5 %fusion.1 = f32[128,8]{0,1:T(8,128)S(1)} fusion(f32[128,8,2048]{2,0,1:T(8,128)S(1)} %get-tuple-element.56, f32[128,8]{0,1:T(8,128)S(1)} %get-tuple-element.55, pred[128,2048]{1,0:T(8,128)(4,1)S(1)} %iota_compare_fusion), kind=kLoop, calls=%fused_computation.3 | loop fusion | flops 10484736 | bytes 8658944 | tf_op jit(solution)/shard_map/reduce_sum | solution.py:345
  136.0 0.7 copy-done.2
  137.0 6.7 %convolution_convert_fusion.2 = bf16[8,128,128]{1,2,0:T(8,128)(2,1)S(1)} fusion(bf16[512,8,128]{0,2,1:T(8,128)(2,1)S(1)} %bitcast.92, f32[128,8]{0,1:T(8,128)S(1)} %fusion.1, f32[128,8,2048]{2,0,1:T(8,128)} %copy-done.2, f32[128,8]{0,1:T(8,128)S(1)} %get-tuple-element.55, pred[128,2048]{1,0:T(8,128)(4,1)S(1)} %iota_compare_fusion, ...), kind=kOutput, calls=%fused_computation.32 | convolution fusion | flops 2293366784 | bytes 12066816 | tf_op jit(solution)/shard_map/thl,lhv->thv/dot_general | solution.py:356
  143.7 0.6 log_add_fusion
  144.7 3.0 %fusion.36 = bf16[512,256]{1,0:T(8,128)(2,1)} fusion(f32[542,256]{1,0:T(8,128)S(1)} %maximum_convert_fusion, f32[256]{0:T(256)S(1)} %bitcast.107, f32[256]{0:T(256)S(1)} %bitcast.108, f32[256]{0:T(256)S(1)} %bitcast.109, f32[256]{0:T(256)S(1)} %bitcast.110, f32[256]{0:T(256)S(1)} %bitcast.111, f32[256]{0:T(256)S(1)} %bitcast.112, f32[256]{0:T(256)S(1)} %bitcast.113, ...), kind=kLoop, calls=%fused_computation.50 | loop fusion | flops 8126464 | bytes 16546816 | tf_op jit(solution)/shard_map/convert_element_type | solution.py:299
  147.7 6.8 %swap_plane.1 = bf16[4,128,256]{2,1,0:T(8,128)(2,1)} custom-call(bf16[4,128,256]{2,1,0:T(8,128)(2,1)} %bitcast.91), custom_call_target="tpu_custom_call" | custom-call | tf_op jit(solution)/shard_map/swap_plane/pallas_call | solution.py:208
  154.5 1.1 convert_reduce_fusion
  155.6 2.5 %all-reduce = (f32[128]{0:T(128)S(1)}, f32[128]{0:T(128)S(1)}) all-reduce(f32[128]{0:T(128)S(1)} %get-tuple-element.11, f32[128]{0:T(128)S(1)} %get-tuple-element.10), channel_id=1, replica_groups=mesh['sp'=16,'tp'=2] {'tp'}, use_global_device_ids=true, to_apply=%region_4.0 | all-reduce | flops 256 | bytes 2048 | tf_op jit(solution)/shard_map/psum | solution.py:301
  158.1 3.3 %convolution_bitcast_fusion = f32[128,2048]{1,0:T(8,128)S(1)} fusion(bf16[4,256,2048]{2,1,0:T(8,128)(2,1)} %bitcast.125, bf16[4,128,256]{2,1,0:T(8,128)(2,1)} %swap_plane.1, f32[4,256]{1,0:T(4,128)S(1)} %mul.592, f32[128]{0:T(128)S(1)} %get-tuple-element.54, f32[128]{0:T(128)S(1)} %get-tuple-element.53), kind=kOutput, calls=%fused_computation.13 | convolution fusion | flops 538050560 | bytes 5510144 | tf_op jit(solution)/shard_map/btc,bcm->tm/dot_general | solution.py:363
  161.6 1.5 fusion.8
  163.2 9.3 %swap_tp.1 = bf16[2,64,2048]{2,1,0:T(8,128)(2,1)} custom-call(bf16[2,64,2048]{2,1,0:T(8,128)(2,1)} %bitcast.86), custom_call_target="tpu_custom_call" | custom-call | tf_op jit(solution)/shard_map/swap_tp/pallas_call | solution.py:208
  172.4 1.9 %reduce_sum.62 = bf16[64,2048]{1,0:T(8,128)(2,1)} reduce(bf16[2,64,2048]{2,1,0:T(8,128)(2,1)} %swap_tp.1, bf16[]{:T(256)} %constant.67.clone.1), dimensions={0}, to_apply=%region_8.9 | reduce | flops 131072 | bytes 786434 | tf_op jit(solution)/shard_map/reduce_sum | solution.py:372
  (112 shorter events, 4.3 us)
Async XLA Ops:
  0.6 91.7 %copy-start = (bf16[512,1024]{1,0:T(8,128)(2,1)S(1)}, bf16[512,1024]{1,0:T(8,128)(2,1)}, u32[]{:S(2)}) copy-start(bf16[512,1024]{1,0:T(8,128)(2,1)} %param.24) | copy-start | bytes 3145732
  72.9 9.9 %copy-start.1 = (bf16[4,128,2048]{2,1,0:T(8,128)(2,1)S(1)}, bf16[4,128,2048]{2,1,0:T(8,128)(2,1)}, u32[]{:S(2)}) copy-start(bf16[4,128,2048]{2,1,0:T(8,128)(2,1)} %get-tuple-element.6) | copy-start | bytes 6291460
  73.0 9.9 %copy-start.8 = (f32[2048]{0:T(1024)S(1)}, f32[2048]{0:T(1024)}, u32[]{:S(2)}) copy-start(f32[2048]{0:T(1024)} %param.15) | copy-start | bytes 24580
  75.0 69.4 %collective-permute-start = (bf16[30,256]{1,0:T(8,128)(2,1)}, bf16[30,256]{1,0:T(8,128)(2,1)S(1)}, u32[]{:S(2)}, u32[]{:S(2)}) collective-permute-start(bf16[30,256]{1,0:T(8,128)(2,1)} %slice.288), channel_id=1, source_target_pairs={{0,8},{2,10},{4,12},{6,14},{8,16},{10,18},{12,20},{14,22},{16,24},... | collective-permute-start | bytes 46088 | tf_op jit(solution)/shard_map/ppermute | solution.py:292
  93.9 34.0 %copy-start.5 = (bf16[128,8,512]{2,0,1:T(8,128)(2,1)S(1)}, bf16[128,8,512]{2,0,1:T(8,128)(2,1)}, u32[]{:S(2)}) copy-start(bf16[128,8,512]{2,0,1:T(8,128)(2,1)} %fusion.9) | copy-start | bytes 3145732
  136.7 7.7 %copy-start.10 = (f32[1,256]{1,0:T(1,128)S(1)}, f32[1,256]{1,0:T(1,128)}, u32[]{:S(2)}) copy-start(f32[1,256]{1,0:T(1,128)} %get-tuple-element.38) | copy-start | bytes 3076
  136.8 7.7 %copy-start.11 = (f32[1,256]{1,0:T(1,128)S(1)}, f32[1,256]{1,0:T(1,128)}, u32[]{:S(2)}) copy-start(f32[1,256]{1,0:T(1,128)} %get-tuple-element.39) | copy-start | bytes 3076
  136.8 7.7 %copy-start.12 = (f32[1,256]{1,0:T(1,128)S(1)}, f32[1,256]{1,0:T(1,128)}, u32[]{:S(2)}) copy-start(f32[1,256]{1,0:T(1,128)} %get-tuple-element.40) | copy-start | bytes 3076
  136.8 7.7 %copy-start.13 = (f32[1,256]{1,0:T(1,128)S(1)}, f32[1,256]{1,0:T(1,128)}, u32[]{:S(2)}) copy-start(f32[1,256]{1,0:T(1,128)} %get-tuple-element.41) | copy-start | bytes 3076
  136.8 7.7 %copy-start.14 = (f32[1,256]{1,0:T(1,128)S(1)}, f32[1,256]{1,0:T(1,128)}, u32[]{:S(2)}) copy-start(f32[1,256]{1,0:T(1,128)} %get-tuple-element.42) | copy-start | bytes 3076
  136.8 7.7 %copy-start.15 = (f32[1,256]{1,0:T(1,128)S(1)}, f32[1,256]{1,0:T(1,128)}, u32[]{:S(2)}) copy-start(f32[1,256]{1,0:T(1,128)} %get-tuple-element.43) | copy-start | bytes 3076
  136.8 7.7 %copy-start.16 = (f32[1,256]{1,0:T(1,128)S(1)}, f32[1,256]{1,0:T(1,128)}, u32[]{:S(2)}) copy-start(f32[1,256]{1,0:T(1,128)} %get-tuple-element.44) | copy-start | bytes 3076
  136.8 7.7 %copy-start.17 = (f32[1,256]{1,0:T(1,128)S(1)}, f32[1,256]{1,0:T(1,128)}, u32[]{:S(2)}) copy-start(f32[1,256]{1,0:T(1,128)} %get-tuple-element.45) | copy-start | bytes 3076
  136.8 7.7 %copy-start.18 = (f32[1,256]{1,0:T(1,128)S(1)}, f32[1,256]{1,0:T(1,128)}, u32[]{:S(2)}) copy-start(f32[1,256]{1,0:T(1,128)} %get-tuple-element.46) | copy-start | bytes 3076
  136.8 7.7 %copy-start.19 = (f32[1,256]{1,0:T(1,128)S(1)}, f32[1,256]{1,0:T(1,128)}, u32[]{:S(2)}) copy-start(f32[1,256]{1,0:T(1,128)} %get-tuple-element.47) | copy-start | bytes 3076
  136.8 7.7 %copy-start.20 = (f32[1,256]{1,0:T(1,128)S(1)}, f32[1,256]{1,0:T(1,128)}, u32[]{:S(2)}) copy-start(f32[1,256]{1,0:T(1,128)} %get-tuple-element.48) | copy-start | bytes 3076
  136.9 7.7 %copy-start.21 = (f32[1,256]{1,0:T(1,128)S(1)}, f32[1,256]{1,0:T(1,128)}, u32[]{:S(2)}) copy-start(f32[1,256]{1,0:T(1,128)} %get-tuple-element.18) | copy-start | bytes 3076
  136.9 7.7 %copy-start.22 = (f32[1,256]{1,0:T(1,128)S(1)}, f32[1,256]{1,0:T(1,128)}, u32[]{:S(2)}) copy-start(f32[1,256]{1,0:T(1,128)} %get-tuple-element.19) | copy-start | bytes 3076
  136.9 7.7 %copy-start.23 = (f32[1,256]{1,0:T(1,128)S(1)}, f32[1,256]{1,0:T(1,128)}, u32[]{:S(2)}) copy-start(f32[1,256]{1,0:T(1,128)} %get-tuple-element.20) | copy-start | bytes 3076
  136.9 7.7 %copy-start.24 = (f32[1,256]{1,0:T(1,128)S(1)}, f32[1,256]{1,0:T(1,128)}, u32[]{:S(2)}) copy-start(f32[1,256]{1,0:T(1,128)} %get-tuple-element.21) | copy-start | bytes 3076
  136.9 7.7 %copy-start.25 = (f32[1,256]{1,0:T(1,128)S(1)}, f32[1,256]{1,0:T(1,128)}, u32[]{:S(2)}) copy-start(f32[1,256]{1,0:T(1,128)} %get-tuple-element.22) | copy-start | bytes 3076
  136.9 7.7 %copy-start.26 = (f32[1,256]{1,0:T(1,128)S(1)}, f32[1,256]{1,0:T(1,128)}, u32[]{:S(2)}) copy-start(f32[1,256]{1,0:T(1,128)} %get-tuple-element.23) | copy-start | bytes 3076
  136.9 7.7 %copy-start.27 = (f32[1,256]{1,0:T(1,128)S(1)}, f32[1,256]{1,0:T(1,128)}, u32[]{:S(2)}) copy-start(f32[1,256]{1,0:T(1,128)} %get-tuple-element.24) | copy-start | bytes 3076
  136.9 7.7 %copy-start.28 = (f32[1,256]{1,0:T(1,128)S(1)}, f32[1,256]{1,0:T(1,128)}, u32[]{:S(2)}) copy-start(f32[1,256]{1,0:T(1,128)} %get-tuple-element.25) | copy-start | bytes 3076
  136.9 7.7 %copy-start.29 = (f32[1,256]{1,0:T(1,128)S(1)}, f32[1,256]{1,0:T(1,128)}, u32[]{:S(2)}) copy-start(f32[1,256]{1,0:T(1,128)} %get-tuple-element.26) | copy-start | bytes 3076
  136.9 7.7 %copy-start.30 = (f32[1,256]{1,0:T(1,128)S(1)}, f32[1,256]{1,0:T(1,128)}, u32[]{:S(2)}) copy-start(f32[1,256]{1,0:T(1,128)} %get-tuple-element.27) | copy-start | bytes 3076
  137.0 7.7 %copy-start.31 = (f32[1,256]{1,0:T(1,128)S(1)}, f32[1,256]{1,0:T(1,128)}, u32[]{:S(2)}) copy-start(f32[1,256]{1,0:T(1,128)} %get-tuple-element.28) | copy-start | bytes 3076
  137.0 7.7 %copy-start.32 = (f32[1,256]{1,0:T(1,128)S(1)}, f32[1,256]{1,0:T(1,128)}, u32[]{:S(2)}) copy-start(f32[1,256]{1,0:T(1,128)} %get-tuple-element.29) | copy-start | bytes 3076
  137.0 7.7 %copy-start.33 = (f32[1,256]{1,0:T(1,128)S(1)}, f32[1,256]{1,0:T(1,128)}, u32[]{:S(2)}) copy-start(f32[1,256]{1,0:T(1,128)} %get-tuple-element.30) | copy-start | bytes 3076
  137.0 7.7 %copy-start.34 = (f32[1,256]{1,0:T(1,128)S(1)}, f32[1,256]{1,0:T(1,128)}, u32[]{:S(2)}) copy-start(f32[1,256]{1,0:T(1,128)} %get-tuple-element.31) | copy-start | bytes 3076
  137.0 7.7 %copy-start.35 = (f32[1,256]{1,0:T(1,128)S(1)}, f32[1,256]{1,0:T(1,128)}, u32[]{:S(2)}) copy-start(f32[1,256]{1,0:T(1,128)} %get-tuple-element.32) | copy-start | bytes 3076
  137.0 7.7 %copy-start.36 = (f32[1,256]{1,0:T(1,128)S(1)}, f32[1,256]{1,0:T(1,128)}, u32[]{:S(2)}) copy-start(f32[1,256]{1,0:T(1,128)} %get-tuple-element.33) | copy-start | bytes 3076
  (16 other events, 89.9 us)
